TPU v7x, 32 devices: a whole 2x2x4 slice. The times are simulated.
32 devices in a mesh: fs: 16 (over z, y, core), tp: 2 (over x).
Axes of the slice: x: 2, y: 2, z: 4, core: 2. Of those that a mesh axis runs over, the one named last changes fastest.
Arguments:
- prompt: bfloat16 [2048, 2048], P('fs'), may hold values from -6 to 6
- norm_gain: float32 [2048], P('fs'), may hold values from 0.1 to 1.9
- gate_train: float32 [2048, 32768], P('fs', 'tp'), may hold values from -0.125 to 0.125
- up_train: float32 [2048, 32768], P('fs', 'tp'), may hold values from -0.125 to 0.125
- down_train: float32 [2048, 32768], P('fs', 'tp'), may hold values from -0.25 to 0.25
- common_gate_train: float32 [2048, 512], P('fs', 'tp'), may hold values from -0.125 to 0.125
- common_up_train: float32 [2048, 512], P('fs', 'tp'), may hold values from -0.125 to 0.125
- common_down_train: float32 [2048, 512], P('fs', 'tp'), may hold values from -0.25 to 0.25
- route_ids: int32 [2048, 6], P('fs'), may hold values from 0 to 63, all different within a row; in each aligned block of 128 rows (0 to 127, 128 to 255, ...) at most 16 rows name the same one
- route_weights: float32 [2048, 6], P('fs'), may hold values from 0.1 to 1
Outputs:
- mixture: bfloat16 [2048, 2048], P('fs', 'tp')
- gate_serve: bfloat16 [64, 512, 2048], P('fs', 'tp')
- up_serve: bfloat16 [64, 512, 2048], P('fs', 'tp')
- down_serve: bfloat16 [64, 512, 2048], P('fs', 'tp')
- common_gate_serve: bfloat16 [512, 2048], P('tp')
- common_up_serve: bfloat16 [512, 2048], P('tp')
- common_down_serve: bfloat16 [512, 2048], P('tp')
Inputs may be any that keep to these rules, and one draw needn't show every extreme that they name: `route_ids`: each row names 6 different experts. Among the rows of one index of fs no expert is named more than 16 times, and in every draw some expert is named exactly 16 times by the rows of some index.
All inputs are finite; a program needn't handle non-finite values.
Results may differ from a plain program's by a relative error of at most 0.011.
Values may be sent and summed in bfloat16 or wider, within the bound.
A program may use at most 128 MiB of HBM per device.

v0:
```python
import jax
import jax.numpy as jnp
from jax import lax
from jax.sharding import PartitionSpec as P

FF = 512
E = 64
TOP_K = 6
CAP = 16


epsilon = 1e-06


def shortened(x):
    return jax.tree.map(lambda a: a.astype(jnp.bfloat16) if a.dtype == jnp.float32 else a, x)


def local(
    prompt,
    norm_gain,
    gate_train,
    up_train,
    down_train,
    common_gate_train,
    common_up_train,
    common_down_train,
    route_ids,
    route_weights,
):
    tp_count = lax.axis_size("tp")
    fs_count = lax.axis_size("fs")
    width_rows = gate_train.shape[0]
    local_experts_tp = gate_train.shape[1] // FF
    unit_block = FF // tp_count
    gain_col = norm_gain[:, None]

    def arrange(low):
        sectioned = low.reshape(width_rows, local_experts_tp, tp_count, unit_block)
        sectioned = jnp.transpose(sectioned, (2, 1, 3, 0))
        return sectioned.reshape(tp_count, local_experts_tp, unit_block * width_rows)

    crossed = (
        lax.all_to_all(
            arrange((gate_train * gain_col).astype(jnp.bfloat16)),
            "tp",
            split_axis=0,
            concat_axis=1,
            tiled=True,
        ),
        lax.all_to_all(
            arrange((up_train * gain_col).astype(jnp.bfloat16)),
            "tp",
            split_axis=0,
            concat_axis=1,
            tiled=True,
        ),
        lax.all_to_all(
            arrange(down_train.astype(jnp.bfloat16)), "tp", split_axis=0, concat_axis=1, tiled=True
        ),
    )
    all_experts = crossed[0].shape[1]
    spread = lax.all_to_all(
        shortened(
            tuple((item.reshape(all_experts, 1, unit_block * width_rows) for item in crossed))
        ),
        "fs",
        split_axis=0,
        concat_axis=1,
        tiled=True,
    )

    def finish(arrived_weights):
        owned = arrived_weights.shape[0]
        sectioned = arrived_weights.reshape(owned, fs_count, unit_block, width_rows)
        return jnp.transpose(sectioned, (0, 2, 1, 3)).reshape(
            owned, unit_block, fs_count * width_rows
        )

    gate_serve, up_serve, down_serve = (finish(item) for item in spread)
    common_block = common_gate_train.shape[1]
    common_low = jnp.stack(
        [
            jnp.transpose(common_gate_train * gain_col),
            jnp.transpose(common_up_train * gain_col),
            jnp.transpose(common_down_train),
        ]
    ).astype(jnp.bfloat16)
    common_all = lax.all_gather(
        common_low.reshape(1, 3 * common_block * width_rows), "fs", axis=0, tiled=True
    )
    common_all = jnp.transpose(
        common_all.reshape(fs_count, 3, common_block, width_rows), (1, 2, 0, 3)
    )
    common_all = common_all.reshape(3, common_block, fs_count * width_rows)
    common_gate_serve, common_up_serve, common_down_serve = (
        common_all[0],
        common_all[1],
        common_all[2],
    )
    values = prompt.astype(jnp.float32)
    normed = (
        values * lax.rsqrt(jnp.mean(values * values, axis=1, keepdims=True) + epsilon)
    ).astype(jnp.bfloat16)
    flat_ids = route_ids.reshape(-1)
    onehot = (flat_ids[:, None] == jnp.arange(E, dtype=jnp.int32)[None, :]).astype(jnp.int32)
    before = jnp.cumsum(onehot, axis=0) - onehot
    slot_of = jnp.sum(before * onehot, axis=1)
    target = flat_ids * CAP + slot_of
    model_width = normed.shape[1]
    buffer = (
        jnp.zeros((E * CAP, model_width), jnp.bfloat16)
        .at[target]
        .set(jnp.repeat(normed, TOP_K, axis=0))
    )
    buffer = buffer.reshape(E, CAP, model_width)
    common_gate = jnp.einsum(
        "td,fd->tf", normed, common_gate_serve, preferred_element_type=jnp.float32
    )
    common_up = jnp.einsum("td,fd->tf", normed, common_up_serve, preferred_element_type=jnp.float32)
    common_hidden = (jax.nn.silu(common_gate) * common_up).astype(jnp.bfloat16)
    common_partial = jnp.dot(
        common_hidden, common_down_serve, preferred_element_type=jnp.float32
    ).astype(jnp.bfloat16)
    whole_gate, whole_up, whole_down = (
        lax.all_gather(gate_serve, "tp", axis=1, tiled=True),
        lax.all_gather(up_serve, "tp", axis=1, tiled=True),
        lax.all_gather(down_serve, "tp", axis=1, tiled=True),
    )
    share = CAP // tp_count
    first_slot = lax.axis_index("tp") * share
    my_slots = lax.dynamic_slice_in_dim(buffer, first_slot, share, 1)
    arrived = lax.all_to_all(my_slots, "fs", split_axis=0, concat_axis=1, tiled=True)
    gate_value = jnp.einsum("erd,efd->erf", arrived, whole_gate, preferred_element_type=jnp.float32)
    up_value = jnp.einsum("erd,efd->erf", arrived, whole_up, preferred_element_type=jnp.float32)
    hidden = (jax.nn.silu(gate_value) * up_value).astype(jnp.bfloat16)
    owned, slot_rows = (hidden.shape[0], hidden.shape[1])
    blocked_hidden = hidden.reshape(owned, slot_rows, tp_count, unit_block)
    blocked_down = whole_down.reshape(owned, tp_count, unit_block, model_width)
    partial_value = jnp.einsum(
        "ermf,emfd->merd", blocked_hidden, blocked_down, preferred_element_type=jnp.float32
    ).astype(jnp.bfloat16)
    expert_out = jnp.sum(partial_value.astype(jnp.float32), axis=0).astype(jnp.bfloat16)
    returned = lax.all_to_all(expert_out, "fs", split_axis=1, concat_axis=0, tiled=True)
    inside = (slot_of >= first_slot) & (slot_of < first_slot + share)
    local_index = jnp.where(inside, flat_ids * share + slot_of - first_slot, 0)
    picked = returned.reshape(E * share, model_width)[local_index].astype(jnp.float32)
    pair_weights = jnp.where(inside, route_weights.reshape(-1), 0.0)
    weighted_part = jnp.sum(
        (picked * pair_weights[:, None]).reshape(-1, TOP_K, model_width), axis=1
    )
    weighted, common_sum = (
        lax.psum_scatter(weighted_part, "tp", scatter_dimension=1, tiled=True),
        lax.psum_scatter(common_partial.astype(jnp.float32), "tp", scatter_dimension=1, tiled=True),
    )
    common_out = common_sum.astype(jnp.bfloat16)
    mixture = (weighted + common_out.astype(jnp.float32)).astype(jnp.bfloat16)
    return (
        mixture,
        gate_serve,
        up_serve,
        down_serve,
        common_gate_serve,
        common_up_serve,
        common_down_serve,
    )


def solution(mesh):
    in_specs = (
        P("fs", None),
        P("fs"),
        P("fs", "tp"),
        P("fs", "tp"),
        P("fs", "tp"),
        P("fs", "tp"),
        P("fs", "tp"),
        P("fs", "tp"),
        P("fs", None),
        P("fs", None),
    )
    out_specs = (
        P("fs", "tp"),
        P("fs", "tp", None),
        P("fs", "tp", None),
        P("fs", "tp", None),
        P("tp", None),
        P("tp", None),
        P("tp", None),
    )
    return jax.shard_map(local, mesh=mesh, in_specs=in_specs, out_specs=out_specs, check_vma=False)
```

profile of v0, /device:TPU:0, one launch (start us, length us, event | category | flops | bytes accessed | tf_op | source)
XLA Modules:
  0.0 861.6 jit_solution(5667237024494821347)
XLA Ops:
  7.2 10.8 %multiply_convert_fusion.1 = (bf16[128,16384]{1,0:T(8,128)(2,1)}, bf16[128,16384]{1,0:T(8,128)(2,1)}) fusion(f32[128,16384]{1,0:T(8,128)} %param.12, f32[128]{0:T(128)} %param.11, f32[128,16384]{1,0:T(8,128)} %param.13), kind=kLoop, calls=%fused_computation.6 | loop fusion | flops 8388608 | bytes 25166336 | tf_op jit(solution)/shard_map/convert_element_type | solution.py:45
  25.7 11.3 %copy.100 = bf16[128,32,2,256]{0,3,1,2:T(8,128)(2,1)} copy(bf16[128,32,2,256]{3,2,1,0:T(2,128)(2,1)} %reshape.235) | data formatting | bytes 8388608 | tf_op jit(solution)/shard_map/reshape | solution.py:39
  63.7 11.3 %copy.108 = bf16[128,32,2,256]{0,3,1,2:T(8,128)(2,1)} copy(bf16[128,32,2,256]{3,2,1,0:T(2,128)(2,1)} %reshape.246) | data formatting | bytes 8388608 | tf_op jit(solution)/shard_map/reshape | solution.py:39
  82.2 16.6 %all-to-all-done.1 = bf16[2,32,32768]{2,1,0:T(8,128)(2,1)} async-done(((bf16[2,32,32768]{2,1,0:T(8,128)(2,1)}), bf16[2,32,32768]{2,1,0:T(8,128)(2,1)}, u32[]{:S(2)}, u32[]{:S(2)}) %all-to-all-start.1) | async-done | bytes 4194336 | tf_op jit(solution)/shard_map/all_to_all | solution.py:44
  104.4 7.8 reshape.240
  112.2 11.3 %copy.104 = bf16[128,32,2,256]{0,3,1,2:T(8,128)(2,1)} copy(bf16[128,32,2,256]{3,2,1,0:T(2,128)(2,1)} %reshape.240) | data formatting | bytes 8388608 | tf_op jit(solution)/shard_map/reshape | solution.py:39
  130.8 20.7 %all-to-all-done.5 = bf16[2,32,32768]{2,1,0:T(8,128)(2,1)} async-done(((bf16[2,32,32768]{2,1,0:T(8,128)(2,1)}), bf16[2,32,32768]{2,1,0:T(8,128)(2,1)}, u32[]{:S(2)}, u32[]{:S(2)}) %all-to-all-start.5) | async-done | bytes 4194336 | tf_op jit(solution)/shard_map/all_to_all | solution.py:58
  164.5 7.8 reshape.287
  172.3 31.1 %all-to-all-done.3 = bf16[2,32,32768]{2,1,0:T(8,128)(2,1)} async-done(((bf16[2,32,32768]{2,1,0:T(8,128)(2,1)}), bf16[2,32,32768]{2,1,0:T(8,128)(2,1)}, u32[]{:S(2)}, u32[]{:S(2)}) %all-to-all-start.3) | async-done | bytes 4194336 | tf_op jit(solution)/shard_map/all_to_all | solution.py:51
  215.9 7.9 reshape.291
  223.8 62.9 %all-to-all-done.6 = bf16[16,2,65536]{2,1,0:T(2,128)(2,1)} async-done(((bf16[16,2,65536]{2,1,0:T(2,128)(2,1)}), bf16[16,2,65536]{2,1,0:T(2,128)(2,1)}, u32[]{:S(2)}, u32[]{:S(2)}) %all-to-all-start.6) | async-done | bytes 4194336 | tf_op jit(solution)/shard_map/all_to_all | solution.py:63
  286.7 19.7 %all-to-all-start.2 = ((bf16[16,2,65536]{2,1,0:T(2,128)(2,1)}), bf16[16,2,65536]{2,1,0:T(2,128)(2,1)}, u32[]{:S(2)}, u32[]{:S(2)}) async-start(bf16[16,2,65536]{2,1,0:T(2,128)(2,1)} %reshape.291), calls=%async_computation.2 | async-start | bytes 8388608 | tf_op jit(solution)/shard_map/all_to_all | solution.py:63
  306.9 12.3 %reshape.288 = bf16[64,1,32768]{2,1,0:T(2,128)(2,1)} reshape(bf16[16,2,65536]{2,1,0:T(2,128)(2,1)} %all-to-all-done.6) | data formatting | bytes 8388608
  319.2 26.1 %reduce.5 = bf16[64,32768]{1,0:T(8,128)(2,1)} reduce(bf16[64,1,32768]{2,1,0:T(2,128)(2,1)} %reshape.288, bf16[]{:T(256)} %constant.38), dimensions={1}, to_apply=%all_to_all.91.reduce_sub_computation | reduce | bytes 8388610 | tf_op jit(solution)/shard_map/all_to_all | solution.py:63
  352.5 8.4 reshape.277
  373.9 8.3 reshape.289
  383.9 19.7 %all-to-all-start.4 = ((bf16[16,2,65536]{2,1,0:T(2,128)(2,1)}), bf16[16,2,65536]{2,1,0:T(2,128)(2,1)}, u32[]{:S(2)}, u32[]{:S(2)}) async-start(bf16[16,2,65536]{2,1,0:T(2,128)(2,1)} %reshape.289), calls=%async_computation.4 | async-start | bytes 8388608 | tf_op jit(solution)/shard_map/all_to_all | solution.py:63
  403.7 12.4 %reshape.292 = bf16[64,1,32768]{2,1,0:T(2,128)(2,1)} reshape(bf16[16,2,65536]{2,1,0:T(2,128)(2,1)} %all-to-all-done.2) | data formatting | bytes 8388608
  416.1 26.1 %reduce.3 = bf16[64,32768]{1,0:T(8,128)(2,1)} reduce(bf16[64,1,32768]{2,1,0:T(2,128)(2,1)} %reshape.292, bf16[]{:T(256)} %constant.38), dimensions={1}, to_apply=%all_to_all.83.reduce_sub_computation | reduce | bytes 8388610 | tf_op jit(solution)/shard_map/all_to_all | solution.py:63
  449.3 8.4 reshape.275
  462.8 18.4 %all-to-all-done.4 = bf16[16,2,65536]{2,1,0:T(2,128)(2,1)} async-done(((bf16[16,2,65536]{2,1,0:T(2,128)(2,1)}), bf16[16,2,65536]{2,1,0:T(2,128)(2,1)}, u32[]{:S(2)}, u32[]{:S(2)}) %all-to-all-start.4) | async-done | bytes 4194336 | tf_op jit(solution)/shard_map/all_to_all | solution.py:63
  481.2 12.7 %reshape.290 = bf16[64,1,32768]{2,1,0:T(2,128)(2,1)} reshape(bf16[16,2,65536]{2,1,0:T(2,128)(2,1)} %all-to-all-done.4) | data formatting | bytes 8388608
  493.9 26.1 %reduce.4 = bf16[64,32768]{1,0:T(8,128)(2,1)} reduce(bf16[64,1,32768]{2,1,0:T(2,128)(2,1)} %reshape.290, bf16[]{:T(256)} %constant.38), dimensions={1}, to_apply=%all_to_all.87.reduce_sub_computation | reduce | bytes 8388610 | tf_op jit(solution)/shard_map/all_to_all | solution.py:63
  527.1 8.4 reshape.276
  553.0 9.4 %scatter_custom_fusion = bf16[1024,2048]{1,0:T(8,128)(2,1)} fusion(s32[768]{0:T(1024)S(1)} %get-tuple-element.29, bf16[768,2048]{1,0:T(8,128)(2,1)S(1)} %reshape.267, bf16[]{:T(256)} %constant.11.clone.1), kind=kCustom, calls=%fused_computation.17 | custom fusion | bytes 4194306 | tf_op jit(solution)/shard_map/scatter | solution.py:114
  565.6 19.3 %all-to-all-start = ((bf16[64,8,2048]{2,1,0:T(8,128)(2,1)}), bf16[64,8,2048]{2,1,0:T(8,128)(2,1)S(1)}, u32[]{:S(2)}, u32[]{:S(2)}) async-start(bf16[64,8,2048]{2,1,0:T(8,128)(2,1)} %constant_dynamic-slice_fusion), calls=%async_computation | async-start | bytes 4194304 | tf_op jit(solution)/shard_map/all_to_all | solution.py:133
  586.4 12.1 %copy.112 = bf16[4,512,2048]{2,1,0:T(8,128)(2,1)} copy(bf16[4,512,2048]{1,2,0:T(8,128)(2,1)} %all-gather.10.cloned.1.call-done) | data formatting | bytes 16777216 | tf_op jit(solution)/shard_map/all_gather | solution.py:128
  598.5 27.4 %all-to-all-done = bf16[64,8,2048]{2,1,0:T(8,128)(2,1)S(1)} async-done(((bf16[64,8,2048]{2,1,0:T(8,128)(2,1)}), bf16[64,8,2048]{2,1,0:T(8,128)(2,1)S(1)}, u32[]{:S(2)}, u32[]{:S(2)}) %all-to-all-start) | async-done | bytes 2097184 | tf_op jit(solution)/shard_map/all_to_all | solution.py:133
  632.2 51.7 %all-gather.8.cloned.1.call-done = bf16[4,512,2048]{2,1,0:T(8,128)(2,1)} async-done(((bf16[4,256,2048]{2,1,0:T(8,128)(2,1)}), bf16[4,512,2048]{2,1,0:T(8,128)(2,1)}) %all-gather.8.cloned.1.call-update) | async-done | bytes 8388624 | tf_op jit(solution)/shard_map/all_gather | solution.py:127
  700.7 79.4 %all-gather.12.cloned.1.call-done = bf16[16,1,98304]{2,1,0:T(2,128)(2,1)} async-done(((bf16[1,1,98304]{2,1,0:T(2,128)(2,1)}), bf16[16,1,98304]{2,1,0:T(2,128)(2,1)}) %all-gather.12.cloned.1.call-update) | async-done | bytes 3145744 | tf_op jit(solution)/shard_map/all_gather | solution.py:89
  780.0 18.5 %reduce.7 = bf16[16,98304]{1,0:T(8,128)(2,1)S(1)} reduce(bf16[16,1,98304]{2,1,0:T(2,128)(2,1)} %all-gather.12.cloned.1.call-done, bf16[]{:T(256)} %constant.38), dimensions={1}, to_apply=%all-gather.reduce_sub_computation | reduce | bytes 6291458 | tf_op jit(solution)/shard_map/all_gather | solution.py:89
  840.3 12.1 %reduce-scatter.3.cloned.1.call-done = f32[128,1024]{1,0:T(8,128)} async-done(((f32[128,2048]{1,0:T(8,128)}), f32[128,1024]{1,0:T(8,128)}) %reduce-scatter.3.cloned.1.call-update) | async-done | bytes 524304 | tf_op jit(solution)/shard_map/reduce_scatter | solution.py:153
  (114 shorter events, 210.5 us)
Async XLA Ops:
  44.4 54.5 %all-to-all-start.1 = ((bf16[2,32,32768]{2,1,0:T(8,128)(2,1)}), bf16[2,32,32768]{2,1,0:T(8,128)(2,1)}, u32[]{:S(2)}, u32[]{:S(2)}) async-start(bf16[2,32,32768]{2,1,0:T(8,128)(2,1)} %reshape.236), calls=%async_computation.1 | async-start | bytes 8388608 | tf_op jit(solution)/shard_map/all_to_all | solution.py:44
  98.8 52.7 %all-to-all-start.5 = ((bf16[2,32,32768]{2,1,0:T(8,128)(2,1)}), bf16[2,32,32768]{2,1,0:T(8,128)(2,1)}, u32[]{:S(2)}, u32[]{:S(2)}) async-start(bf16[2,32,32768]{2,1,0:T(8,128)(2,1)} %reshape.247), calls=%async_computation.5 | async-start | bytes 8388608 | tf_op jit(solution)/shard_map/all_to_all | solution.py:58
  151.5 51.9 %all-to-all-start.3 = ((bf16[2,32,32768]{2,1,0:T(8,128)(2,1)}), bf16[2,32,32768]{2,1,0:T(8,128)(2,1)}, u32[]{:S(2)}, u32[]{:S(2)}) async-start(bf16[2,32,32768]{2,1,0:T(8,128)(2,1)} %reshape.241), calls=%async_computation.3 | async-start | bytes 8388608 | tf_op jit(solution)/shard_map/all_to_all | solution.py:51
  203.4 83.3 %all-to-all-start.6 = ((bf16[16,2,65536]{2,1,0:T(2,128)(2,1)}), bf16[16,2,65536]{2,1,0:T(2,128)(2,1)}, u32[]{:S(2)}, u32[]{:S(2)}) async-start(bf16[16,2,65536]{2,1,0:T(2,128)(2,1)} %reshape.287), calls=%async_computation.6 | async-start | bytes 8388608 | tf_op jit(solution)/shard_map/all_to_all | solution.py:63
  286.7 97.2 %all-to-all-start.2 = ((bf16[16,2,65536]{2,1,0:T(2,128)(2,1)}), bf16[16,2,65536]{2,1,0:T(2,128)(2,1)}, u32[]{:S(2)}, u32[]{:S(2)}) async-start(bf16[16,2,65536]{2,1,0:T(2,128)(2,1)} %reshape.291), calls=%async_computation.2 | async-start | bytes 8388608 | tf_op jit(solution)/shard_map/all_to_all | solution.py:63
  306.4 280.0 %all-gather.10.cloned.1.call-start = ((), (), s32[]{:S(2)}) async-start(), calls=%async_computation.12 | async-start | bytes 12582912 | tf_op jit(solution)/shard_map/all_gather | solution.py:128
  383.9 97.2 %all-to-all-start.4 = ((bf16[16,2,65536]{2,1,0:T(2,128)(2,1)}), bf16[16,2,65536]{2,1,0:T(2,128)(2,1)}, u32[]{:S(2)}, u32[]{:S(2)}) async-start(bf16[16,2,65536]{2,1,0:T(2,128)(2,1)} %reshape.289), calls=%async_computation.4 | async-start | bytes 8388608 | tf_op jit(solution)/shard_map/all_to_all | solution.py:63
  403.6 222.3 %all-gather.6.cloned.1.call-start = ((), (), s32[]{:S(2)}) async-start(), calls=%async_computation.10 | async-start | bytes 12582912 | tf_op jit(solution)/shard_map/all_gather | solution.py:126
  462.6 221.3 %all-gather.8.cloned.1.call-start = ((), (), s32[]{:S(2)}) async-start(), calls=%async_computation.11 | async-start | bytes 12582912 | tf_op jit(solution)/shard_map/all_gather | solution.py:127
  540.4 0.7 copy-start.10
  540.4 3.7 copy-start.6
  544.5 0.8 copy-start.5
  562.5 22.7 %copy-start.7 = (f32[128,256]{1,0:T(8,128)S(1)}, f32[128,256]{1,0:T(8,128)}, u32[]{:S(2)}) copy-start(f32[128,256]{1,0:T(8,128)} %param.15) | copy-start | bytes 393220
  562.5 22.7 %copy-start.8 = (f32[128,256]{1,0:T(8,128)S(1)}, f32[128,256]{1,0:T(8,128)}, u32[]{:S(2)}) copy-start(f32[128,256]{1,0:T(8,128)} %param.16) | copy-start | bytes 393220
  562.5 22.7 %copy-start.9 = (f32[128,256]{1,0:T(8,128)S(1)}, f32[128,256]{1,0:T(8,128)}, u32[]{:S(2)}) copy-start(f32[128,256]{1,0:T(8,128)} %param.17) | copy-start | bytes 393220
  562.5 22.8 %copy-start.12 = (f32[128]{0:T(128)S(1)}, f32[128]{0:T(128)}, u32[]{:S(2)}) copy-start(f32[128]{0:T(128)} %param.11) | copy-start | bytes 1540
  565.6 60.2 %all-to-all-start = ((bf16[64,8,2048]{2,1,0:T(8,128)(2,1)}), bf16[64,8,2048]{2,1,0:T(8,128)(2,1)S(1)}, u32[]{:S(2)}, u32[]{:S(2)}) async-start(bf16[64,8,2048]{2,1,0:T(8,128)(2,1)} %constant_dynamic-slice_fusion), calls=%async_computation | async-start | bytes 4194304 | tf_op jit(solution)/shard_map/all_to_all | solution.py:133
  584.9 195.1 %all-gather.12.cloned.1.call-start = ((), (), s32[]{:S(2)}) async-start(), calls=%async_computation.15 | async-start | bytes 6684672 | tf_op jit(solution)/shard_map/all_gather | solution.py:89
  683.9 6.5 copy-start.4
  694.7 113.8 %all-to-all-start.7 = ((bf16[4,128,2048]{2,0,1:T(4,128)(2,1)}), bf16[4,128,2048]{2,0,1:T(4,128)(2,1)}, u32[]{:S(2)}, u32[]{:S(2)}) async-start(bf16[4,128,2048]{2,0,1:T(4,128)(2,1)} %copy.115), calls=%async_computation.7 | async-start | bytes 4194304 | tf_op jit(solution)/shard_map/all_to_all | solution.py:144
  700.4 140.0 %reduce-scatter.5.cloned.1.call-start = ((), (), s32[]{:S(2)}) async-start(), calls=%async_computation.14 | async-start | bytes 1572864 | tf_op jit(solution)/shard_map/reduce_scatter | solution.py:154
  801.4 6.7 copy-start
  801.4 6.9 copy-start.11
  803.3 7.9 copy-start.2
  808.1 44.3 %reduce-scatter.3.cloned.1.call-start = ((), (), s32[]{:S(2)}) async-start(), calls=%async_computation.13 | async-start | bytes 1572864 | tf_op jit(solution)/shard_map/reduce_scatter | solution.py:153
  822.2 9.1 %copy-start.1 = (bf16[1,256,16,128]{1,3,2,0:T(8,128)(2,1)S(1)}, bf16[1,256,16,128]{1,3,2,0:T(8,128)(2,1)}, u32[]{:S(2)}) copy-start(bf16[1,256,16,128]{1,3,2,0:T(8,128)(2,1)} %copy-done) | copy-start | bytes 3145732
  829.8 2.9 copy-start.3
Sparse Core Ops, SparseCore 0:
  367.3 104.2 all-gather.9
  473.7 103.9 all-gather.5
  579.8 103.9 all-gather.7
  686.6 93.4 all-gather.11
  808.2 21.5 reduce-scatter.4
  831.9 20.3 reduce-scatter.2
where the time goes:
time: 875 us; the launch traced here: 862 us
  waiting for transfers between devices  322 us (37%)
  local copies, waits for them, and re-layouts  272 us (31%)
  other arithmetic  146 us (17%)
  starting transfers between devices  88.3 us (10%)
  matrix products  18.9 us (2%)
  between operations  15 us (2%)
    all_to_all x3, waiting for transfers between devices, local(): lax.all_to_all(shortened(tuple((item.reshape(all_experts, 1, unit_block *...  82.9 us
    all_gather x1, waiting for transfers between devices, local(): lax.all_gather(common_low.reshape(1, 3 * common_block * width_rows), 'fs'...  79.4 us
    all_to_all x3, other arithmetic, local(): lax.all_to_all(shortened(tuple((item.reshape(all_experts, 1, unit_block *...  78.3 us
    unnamed x40, local copies, waits for them, and re-layouts  75 us
    reshape x6, local copies, waits for them, and re-layouts, arrange(): sectioned = low.reshape(width_rows, local_experts_tp, tp_count, unit_block)  57.2 us
    all_gather x1, waiting for transfers between devices, local(): lax.all_gather(up_serve, 'tp', axis=1, tiled=True)  51.7 us
    all_to_all x3, starting transfers between devices, local(): lax.all_to_all(shortened(tuple((item.reshape(all_experts, 1, unit_block *...  45.1 us
    all_to_all x1, waiting for transfers between devices, local(): lax.all_to_all(arrange((up_train * gain_col).astype(jnp.bfloat16)), 'tp',...  31.1 us
  transfers between devices with their start and end apart: 14, of which 10 were waited for; matrix products, arithmetic and copies ran while one was open for 43% of the time, Pallas kernels for 0%

commit v1 on v0

v1 whole, which is shorter than its diff:
```python
import functools

import jax
import jax.numpy as jnp
from jax import lax
from jax.experimental import pallas as pl
from jax.experimental.pallas import tpu as pltpu
from jax.sharding import PartitionSpec as P

FF = 512
E = 64
TOP_K = 6
CAP = 16
LANES = 128

epsilon = 1e-06


def silu_product(gate_value, up_value):
    return (gate_value / (1.0 + jnp.exp(-gate_value)) * up_value).astype(jnp.bfloat16)


def arrange_kernel(tp_count, chunk, unit_block, scaled, weight_ref, gain_ref, out_ref):
    for i in range(chunk):
        for p in range(tp_count):
            first = (i * tp_count + p) * unit_block
            block = weight_ref[:, first:first + unit_block]
            if scaled:
                block = block * gain_ref[...]
            out_ref[p, 0, i] = block.T.astype(jnp.bfloat16)


def arrange(weight, gain_col, scaled, tp_count, owned, chunks, which):
    width_rows = weight.shape[0]
    unit_block = FF // tp_count
    groups = weight.shape[1] // FF // owned
    chunk = owned // chunks
    if width_rows % LANES:
        low = (weight * gain_col if scaled else weight).astype(jnp.bfloat16)
        low = low.reshape(width_rows, groups, chunks, chunk, tp_count, unit_block)[:, :, which]
        return jnp.transpose(low, (3, 1, 2, 4, 0))
    out = jax.ShapeDtypeStruct((tp_count, groups, chunk, unit_block, width_rows), jnp.bfloat16)
    size = groups * chunk * FF * width_rows
    return pl.pallas_call(
        functools.partial(arrange_kernel, tp_count, chunk, unit_block, scaled),
        grid=(groups,),
        in_specs=[
            pl.BlockSpec((width_rows, chunk * FF), lambda j: (0, j * chunks + which)),
            pl.BlockSpec((width_rows, 1), lambda j: (0, 0)),
        ],
        out_specs=pl.BlockSpec((tp_count, 1, chunk, unit_block, width_rows), lambda j: (0, j, 0, 0, 0)),
        out_shape=out,
        cost_estimate=pl.CostEstimate(flops=size, bytes_accessed=6 * size, transcendentals=0),
    )(weight, gain_col)


def cross(blocks):
    tp_count = lax.axis_size("tp")
    me = lax.axis_index("tp")
    arrived = blocks
    for shift in range(1, tp_count):
        sent = lax.dynamic_index_in_dim(blocks, lax.rem(me + shift, tp_count), 0, keepdims=True)
        got = lax.ppermute(sent, "tp", [(i, (i + shift) % tp_count) for i in range(tp_count)])
        arrived = lax.dynamic_update_slice_in_dim(arrived, got, lax.rem(me - shift + tp_count, tp_count), 0)
    return arrived


def dot_t(a, b):
    return lax.dot_general(a, b, (((1,), (1,)), ((), ())), preferred_element_type=jnp.float32)


def first_kernel(sources, width_rows, rows_ref, gate_ref, up_ref, *rest):
    gate_out, up_out, hidden_ref = rest[-3:]
    for s in range(sources):
        columns = slice(s * width_rows, (s + 1) * width_rows)
        gate_out[0, :, columns] = gate_ref[s, 0]
        up_out[0, :, columns] = up_ref[s, 0]
    rows = rows_ref[0]
    hidden_ref[0] = silu_product(dot_t(rows, gate_out[0]), dot_t(rows, up_out[0]))


def second_kernel(sources, width_rows, tp_count, hidden_ref, down_ref, *rest):
    down_out, partial_ref = rest[-2:]
    for s in range(sources):
        down_out[0, :, s * width_rows:(s + 1) * width_rows] = down_ref[s, 0]
    result = jnp.dot(hidden_ref[0], down_out[0], preferred_element_type=jnp.float32).astype(jnp.bfloat16)
    share = result.shape[1] // tp_count
    for p in range(tp_count):
        for b in range(result.shape[0] // CAP):
            partial_ref[p, b, 0] = result[b * CAP:(b + 1) * CAP, p * share:(p + 1) * share]


def joined(arrived):
    sources, chunk, unit_block, width_rows = arrived.shape
    return jnp.transpose(arrived, (1, 2, 0, 3)).reshape(chunk, unit_block, sources * width_rows)


def expert_first(rows, gate, up, before, owned, which):
    sources, chunk, unit_block, width_rows = gate.shape
    slot_rows, width = rows.shape[1], rows.shape[2]
    serve = jax.ShapeDtypeStruct((owned, unit_block, width), jnp.bfloat16)
    weight_spec = pl.BlockSpec((sources, 1, unit_block, width_rows), lambda i: (0, i, 0, 0))
    serve_spec = pl.BlockSpec((1, unit_block, width), lambda i: (which * chunk + i, 0, 0))
    size = chunk * unit_block * width
    return pl.pallas_call(
        functools.partial(first_kernel, sources, width_rows),
        grid=(chunk,),
        in_specs=[pl.BlockSpec((1, slot_rows, width), lambda i: (i, 0, 0)), weight_spec, weight_spec]
        + [pl.BlockSpec(memory_space=pl.ANY)] * len(before),
        out_specs=[serve_spec, serve_spec, pl.BlockSpec((1, slot_rows, unit_block), lambda i: (i, 0, 0))],
        out_shape=[serve, serve, jax.ShapeDtypeStruct((chunk, slot_rows, unit_block), jnp.bfloat16)],
        input_output_aliases={3 + n: n for n in range(len(before))},
        cost_estimate=pl.CostEstimate(flops=4 * size * slot_rows, bytes_accessed=10 * size, transcendentals=0),
    )(rows, gate, up, *before)


def expert_second(hidden, down, before, owned, which, tp_count):
    sources, chunk, unit_block, width_rows = down.shape
    slot_rows = hidden.shape[1]
    width = sources * width_rows
    share = width // tp_count
    blocks = slot_rows // CAP
    size = chunk * unit_block * width
    return pl.pallas_call(
        functools.partial(second_kernel, sources, width_rows, tp_count),
        grid=(chunk,),
        in_specs=[
            pl.BlockSpec((1, slot_rows, unit_block), lambda i: (i, 0, 0)),
            pl.BlockSpec((sources, 1, unit_block, width_rows), lambda i: (0, i, 0, 0)),
        ]
        + [pl.BlockSpec(memory_space=pl.ANY)] * len(before),
        out_specs=[
            pl.BlockSpec((1, unit_block, width), lambda i: (which * chunk + i, 0, 0)),
            pl.BlockSpec((tp_count, blocks, 1, CAP, share), lambda i: (0, 0, i, 0, 0)),
        ],
        out_shape=[
            jax.ShapeDtypeStruct((owned, unit_block, width), jnp.bfloat16),
            jax.ShapeDtypeStruct((tp_count, blocks, chunk, CAP, share), jnp.bfloat16),
        ],
        input_output_aliases={2 + n: n for n in range(len(before))},
        cost_estimate=pl.CostEstimate(flops=2 * size * slot_rows, bytes_accessed=6 * size, transcendentals=0),
    )(hidden, down, *before)


def summed(partials):
    return jnp.sum(partials.astype(jnp.float32), axis=0).astype(jnp.bfloat16)


def local(
    prompt,
    norm_gain,
    gate_train,
    up_train,
    down_train,
    common_gate_train,
    common_up_train,
    common_down_train,
    route_ids,
    route_weights,
):
    tp_count = lax.axis_size("tp")
    fs_count = lax.axis_size("fs")
    me_tp, me_fs = lax.axis_index("tp"), lax.axis_index("fs")
    width_rows = gate_train.shape[0]
    width = width_rows * fs_count
    share = width // tp_count
    unit_block = FF // tp_count
    owned = E // fs_count
    tiled = width_rows % LANES == 0
    chunks = 2 if owned % 2 == 0 else 1
    chunk = owned // chunks
    tokens = prompt.shape[0]
    gain_col = norm_gain[:, None]

    values = prompt.astype(jnp.float32)
    normed = (
        values * lax.rsqrt(jnp.mean(values * values, axis=1, keepdims=True) + epsilon)
    ).astype(jnp.bfloat16)
    named = route_ids[:, :, None] == jnp.arange(E, dtype=jnp.int32)
    named_rows = jnp.any(named, axis=1).astype(jnp.bfloat16)
    earlier = jnp.tril(jnp.ones((tokens, tokens), jnp.bfloat16), -1)
    count = jnp.dot(earlier, named_rows, preferred_element_type=jnp.float32)
    slot_of = jnp.sum(jnp.where(named, count[:, None, :], 0.0), axis=2)
    marks = jnp.concatenate([route_ids.astype(jnp.bfloat16), slot_of.astype(jnp.bfloat16)], axis=1)
    marks = jnp.pad(marks, ((0, 0), (0, LANES - 2 * TOP_K)))
    part = tokens // tp_count
    mine = lax.dynamic_slice_in_dim(jnp.concatenate([normed, marks], axis=1), me_tp * part, part, 0)
    all_rows = lax.all_gather(mine, ("fs", "tp"), axis=0, tiled=True)
    all_rows = all_rows.reshape(fs_count, tokens, width + LANES)
    all_marks = all_rows[:, :, width:].astype(jnp.int32)
    all_ids, all_slots = all_marks[:, :, :TOP_K], all_marks[:, :, TOP_K:2 * TOP_K]
    only_rows = all_rows[:, :, :width]

    def slot_rows_of(which):
        experts = me_fs * owned + which * chunk + jnp.arange(chunk, dtype=jnp.int32)
        slots = jnp.arange(CAP, dtype=jnp.int32)
        chosen = jnp.zeros((fs_count, chunk, CAP, tokens), jnp.bool_)
        for k in range(TOP_K):
            ids_k, slots_k = all_ids[:, None, None, :, k], all_slots[:, None, None, :, k]
            chosen |= (ids_k == experts[None, :, None, None]) & (slots_k == slots[None, None, :, None])
        picked = jnp.einsum(
            "best,btd->besd", chosen.astype(jnp.bfloat16), only_rows, preferred_element_type=jnp.float32
        ).astype(jnp.bfloat16)
        return jnp.transpose(picked, (1, 0, 2, 3)).reshape(chunk, fs_count * CAP, width)

    common_low = jnp.concatenate(
        [
            jnp.transpose(common_gate_train * gain_col),
            jnp.transpose(common_up_train * gain_col),
            jnp.transpose(common_down_train),
        ],
        axis=0,
    ).astype(jnp.bfloat16)
    common_all = lax.all_gather(common_low, "fs", axis=0, tiled=False)
    common_all = jnp.transpose(common_all, (1, 0, 2)).reshape(3, unit_block, width)
    common_gate_serve, common_up_serve, common_down_serve = common_all[0], common_all[1], common_all[2]
    common_hidden = silu_product(dot_t(normed, common_gate_serve), dot_t(normed, common_up_serve))
    common_partial = jnp.dot(
        common_hidden, common_down_serve, preferred_element_type=jnp.float32
    ).astype(jnp.bfloat16)
    common_blocks = jnp.transpose(common_partial.reshape(tokens, tp_count, share), (1, 0, 2))
    common_out = summed(cross(common_blocks)).astype(jnp.float32)

    def finish_chunk(which, partial, mixed):
        expert_out = summed(cross(partial))
        returned = lax.all_to_all(expert_out, "fs", split_axis=0, concat_axis=0, tiled=True)
        returned = returned.reshape(fs_count * chunk * CAP, share)
        place = jnp.arange(fs_count * chunk * CAP, dtype=jnp.int32)
        source, rest = place // (chunk * CAP), place % (chunk * CAP)
        expert_at = source * owned + which * chunk + rest // CAP
        slot_at = rest % CAP
        slots_here = slot_of.astype(jnp.int32)
        spread_weights = jnp.zeros((tokens, place.shape[0]), jnp.float32)
        for k in range(TOP_K):
            hit = (route_ids[:, k:k + 1] == expert_at[None, :]) & (slots_here[:, k:k + 1] == slot_at[None, :])
            spread_weights += jnp.where(hit, route_weights[:, k:k + 1], 0.0)
        left = spread_weights
        for _ in range(3):
            piece = lax.reduce_precision(left, 8, 7)
            left = left - piece
            mixed = mixed + jnp.dot(
                piece.astype(jnp.bfloat16), returned, preferred_element_type=jnp.float32
            )
        return mixed

    def spread(weight, scaled, which, ahead=()):
        crossed = cross(arrange(weight, gain_col, scaled, tp_count, owned, chunks, which))
        crossed = crossed.reshape(fs_count, chunk, unit_block, width_rows)
        if ahead:
            crossed, *ahead = lax.optimization_barrier((crossed, *ahead))
        return lax.all_to_all(crossed, "fs", split_axis=0, concat_axis=0, tiled=True), *ahead

    serves, downs, gates_list = (), (), []
    mixed = common_out
    rows_of = [slot_rows_of(which) for which in range(chunks)]
    for which in range(chunks):
        gate, = spread(gate_train, True, which)
        if which > 0:
            up, mixed, hidden = spread(up_train, True, which, (mixed, hidden))
            down, partial = spread(down_train, False, which, (partial,))
        else:
            up, = spread(up_train, True, which)
            down, = spread(down_train, False, which)
        rows = rows_of[which]
        if which > 0:
            mixed = finish_chunk(which - 1, partial, mixed)
        if tiled:
            gate_serve, up_serve, hidden = expert_first(rows, gate, up, serves, owned, which)
            serves = (gate_serve, up_serve)
            down_serve, partial = expert_second(hidden, down, downs, owned, which, tp_count)
            downs = (down_serve,)
        else:
            whole = joined(gate), joined(up), joined(down)
            gates_list.append(whole)
            hidden = silu_product(
                jnp.einsum("erd,efd->erf", rows, whole[0], preferred_element_type=jnp.float32),
                jnp.einsum("erd,efd->erf", rows, whole[1], preferred_element_type=jnp.float32),
            )
            partial = jnp.einsum(
                "erf,efd->erd", hidden, whole[2], preferred_element_type=jnp.float32
            ).astype(jnp.bfloat16)
            partial = partial.reshape(chunk, fs_count, CAP, tp_count, share)
            partial = jnp.transpose(partial, (3, 1, 0, 2, 4))
    mixed = finish_chunk(chunks - 1, partial, mixed)
    if not tiled:
        gate_serve, up_serve, down_serve = (
            jnp.concatenate([item[n] for item in gates_list], axis=0) for n in range(3)
        )
    return (
        mixed.astype(jnp.bfloat16),
        gate_serve,
        up_serve,
        down_serve,
        common_gate_serve,
        common_up_serve,
        common_down_serve,
    )


def solution(mesh):
    in_specs = (
        P("fs", None),
        P("fs"),
        P("fs", "tp"),
        P("fs", "tp"),
        P("fs", "tp"),
        P("fs", "tp"),
        P("fs", "tp"),
        P("fs", "tp"),
        P("fs", None),
        P("fs", None),
    )
    out_specs = (
        P("fs", "tp"),
        P("fs", "tp", None),
        P("fs", "tp", None),
        P("fs", "tp", None),
        P("tp", None),
        P("tp", None),
        P("tp", None),
    )
    return jax.shard_map(local, mesh=mesh, in_specs=in_specs, out_specs=out_specs, check_vma=False)
```

time: 875 us -> 526 us (0.60); the launches traced: 862 us -> 522 us
  local copies, waits for them, and re-layouts: 272 us -> 53.2 us
  other arithmetic: 146 us -> 13.7 us
  waiting for transfers between devices: 322 us -> 264 us
  Pallas kernels: 0 us -> 57.6 us
  starting transfers between devices: 88.3 us -> 98.2 us
    ppermute x0 -> x9, waiting for transfers between devices: none -> 194 us  [cross(): lax.ppermute(sent, 'tp', [(i, (i + shift) % tp_count) for i in range(tp_c...]
    all_gather x4 -> x2, waiting for transfers between devices: 131 us -> 0.01 us  [the longest x1 0.01 us: local(): common_all = lax.all_gather(common_low, 'fs', axis=0, tiled=False)]
    reshape x16 -> x1, local copies, waits for them, and re-layouts: 119 us -> 0.38 us  [local(): common_partial.reshape(tokens, tp_count, share)]
    all_to_all x8, waiting for transfers between devices: 179 us -> 70.3 us  [the longest x6 57.4 us: spread(): lax.all_to_all(crossed, 'fs', split_axis=0, concat_axis=0, tiled=True)]
    all_to_all x3 -> x0, other arithmetic: 78.3 us -> none  [local(): lax.all_to_all(shortened(tuple((item.reshape(all_experts, 1, unit_block *...]
    unnamed x40 -> x39, local copies, waits for them, and re-layouts: 75 us -> 13.6 us
    pallas_call x0 -> x10, Pallas kernels: none -> 57.6 us  [the longest x6 40.7 us: arrange(): pl.pallas_call(functools.partial(arrange_kernel, tp_count, chunk, unit_bl...]
    all_to_all x5 -> x0, local copies, waits for them, and re-layouts: 24.3 us -> none  [the longest x3 21.4 us: local(): lax.all_to_all(shortened(tuple((item.reshape(all_experts, 1, unit_block *...]
  transfers between devices with their start and end apart: 14 -> 19, of which waited for: 10 -> 15; matrix products, arithmetic and copies ran while one was open for 43% -> 14% of each run, Pallas kernels for 0% -> 11%
where the time goes in v1:
time: 526 us; the launch traced here: 522 us
  waiting for transfers between devices  264 us (50%)
  starting transfers between devices  98.2 us (19%)
  Pallas kernels  57.6 us (11%)
  local copies, waits for them, and re-layouts  53.2 us (10%)
  matrix products  20.6 us (4%)
  between operations  14.5 us (3%)
  other arithmetic  13.7 us (3%)
    ppermute x9, waiting for transfers between devices, cross(): lax.ppermute(sent, 'tp', [(i, (i + shift) % tp_count) for i in range(tp_c...  194 us
    all_to_all x6, starting transfers between devices, spread(): lax.all_to_all(crossed, 'fs', split_axis=0, concat_axis=0, tiled=True)  65.8 us
    all_to_all x6, waiting for transfers between devices, spread(): lax.all_to_all(crossed, 'fs', split_axis=0, concat_axis=0, tiled=True)  57.4 us
    pallas_call x6, Pallas kernels, arrange(): pl.pallas_call(functools.partial(arrange_kernel, tp_count, chunk, unit_bl...  40.7 us
    all_to_all x2, starting transfers between devices, finish_chunk(): lax.all_to_all(expert_out, 'fs', split_axis=0, concat_axis=0, tiled=True)  17.2 us
    ppermute x9, starting transfers between devices, cross(): lax.ppermute(sent, 'tp', [(i, (i + shift) % tp_count) for i in range(tp_c...  15.1 us
    unnamed x39, local copies, waits for them, and re-layouts  13.6 us
    all_to_all x2, waiting for transfers between devices, finish_chunk(): lax.all_to_all(expert_out, 'fs', split_axis=0, concat_axis=0, tiled=True)  12.9 us
  transfers between devices with their start and end apart: 19, of which 15 were waited for; matrix products, arithmetic and copies ran while one was open for 14% of the time, Pallas kernels for 11%

profile of v1, /device:TPU:0, one launch (start us, length us, event | category | flops | bytes accessed | tf_op | source)
XLA Modules:
  0.0 522.3 jit_solution(2222635467949482598)
XLA Ops:
  17.0 6.9 %shard_map.154 = bf16[2,8,2,256,128]{4,3,2,1,0:T(8,128)(2,1)} custom-call(f32[128,16384]{1,0:T(8,128)} %weight_ref.11, f32[128,1]{1,0:T(8,128)} %copy.80.gain_ref), custom_call_target="tpu_custom_call" | custom-call | flops 1048576 | bytes 6291456 | tf_op jit(solution)/shard_map/pallas_call | solution.py:44
  28.2 23.2 %collective-permute-done.2 = bf16[1,8,2,256,128]{4,3,2,1,0:T(8,128)(2,1)S(1)} collective-permute-done((bf16[1,8,2,256,128]{4,3,2,1,0:T(8,128)(2,1)S(1)}, bf16[1,8,2,256,128]{4,3,2,1,0:T(8,128)(2,1)S(1)}, u32[]{:S(2)}, u32[]{:S(2)}) %collective-permute-start.2) | collective-permute-done | bytes 1048608 | tf_op jit(solution)/shard_map/ppermute | solution.py:63
  52.5 6.2 %all-to-all-start = ((bf16[16,2,256,128]{3,2,1,0:T(8,128)(2,1)}), bf16[16,2,256,128]{3,2,1,0:T(8,128)(2,1)S(1)}, u32[]{:S(2)}, u32[]{:S(2)}) async-start(bf16[16,2,256,128]{3,2,1,0:T(8,128)(2,1)} %bitcast.19), calls=%async_computation | async-start | bytes 4194304 | tf_op jit(solution)/shard_map/all_to_all | solution.py:251
  58.6 6.9 %shard_map.155 = bf16[2,8,2,256,128]{4,3,2,1,0:T(8,128)(2,1)} custom-call(f32[128,16384]{1,0:T(8,128)} %weight_ref.8, f32[128,1]{1,0:T(8,128)} %copy.80.gain_ref), custom_call_target="tpu_custom_call" | custom-call | flops 1048576 | bytes 6291456 | tf_op jit(solution)/shard_map/pallas_call | solution.py:44
  68.4 26.0 %collective-permute-done.3 = bf16[1,8,2,256,128]{4,3,2,1,0:T(8,128)(2,1)S(1)} collective-permute-done((bf16[1,8,2,256,128]{4,3,2,1,0:T(8,128)(2,1)S(1)}, bf16[1,8,2,256,128]{4,3,2,1,0:T(8,128)(2,1)S(1)}, u32[]{:S(2)}, u32[]{:S(2)}) %collective-permute-start.3) | collective-permute-done | bytes 1048608 | tf_op jit(solution)/shard_map/ppermute | solution.py:63
  95.4 12.9 %all-to-all-done.gate_ref = bf16[16,2,256,128]{3,2,1,0:T(8,128)(2,1)S(1)} async-done(((bf16[16,2,256,128]{3,2,1,0:T(8,128)(2,1)}), bf16[16,2,256,128]{3,2,1,0:T(8,128)(2,1)S(1)}, u32[]{:S(2)}, u32[]{:S(2)}) %all-to-all-start) | async-done | bytes 2097184 | tf_op jit(solution)/shard_map/all_to_all | solution.py:251
  109.6 20.4 %all-to-all-start.1 = ((bf16[16,2,256,128]{3,2,1,0:T(8,128)(2,1)}), bf16[16,2,256,128]{3,2,1,0:T(8,128)(2,1)}, u32[]{:S(2)}, u32[]{:S(2)}) async-start(bf16[16,2,256,128]{3,2,1,0:T(8,128)(2,1)} %bitcast.20), calls=%async_computation.1 | async-start | bytes 4194304 | tf_op jit(solution)/shard_map/all_to_all | solution.py:251
  130.1 6.9 %shard_map.160 = bf16[2,8,2,256,128]{4,3,2,1,0:T(8,128)(2,1)} custom-call(f32[128,16384]{1,0:T(8,128)} %weight_ref.11, f32[128,1]{1,0:T(8,128)} %copy.80.gain_ref), custom_call_target="tpu_custom_call" | custom-call | flops 1048576 | bytes 6291456 | tf_op jit(solution)/shard_map/pallas_call | solution.py:44
  139.8 27.0 %collective-permute-done.7 = bf16[1,8,2,256,128]{4,3,2,1,0:T(8,128)(2,1)S(1)} collective-permute-done((bf16[1,8,2,256,128]{4,3,2,1,0:T(8,128)(2,1)S(1)}, bf16[1,8,2,256,128]{4,3,2,1,0:T(8,128)(2,1)S(1)}, u32[]{:S(2)}, u32[]{:S(2)}) %collective-permute-start.7) | collective-permute-done | bytes 1048608 | tf_op jit(solution)/shard_map/ppermute | solution.py:63
  167.9 22.9 %all-to-all-done.1.up_ref = bf16[16,2,256,128]{3,2,1,0:T(8,128)(2,1)} async-done(((bf16[16,2,256,128]{3,2,1,0:T(8,128)(2,1)}), bf16[16,2,256,128]{3,2,1,0:T(8,128)(2,1)}, u32[]{:S(2)}, u32[]{:S(2)}) %all-to-all-start.1) | async-done | bytes 2097184 | tf_op jit(solution)/shard_map/all_to_all | solution.py:251
  190.8 11.0 %all-to-all-start.4 = ((bf16[16,2,256,128]{3,2,1,0:T(8,128)(2,1)}), bf16[16,2,256,128]{3,2,1,0:T(8,128)(2,1)S(1)}, u32[]{:S(2)}, u32[]{:S(2)}) async-start(bf16[16,2,256,128]{3,2,1,0:T(8,128)(2,1)} %bitcast.45), calls=%async_computation.4 | async-start | bytes 4194304 | tf_op jit(solution)/shard_map/all_to_all | solution.py:251
  201.7 6.5 %shard_map.158 = bf16[2,8,2,256,128]{4,3,2,1,0:T(8,128)(2,1)} custom-call(f32[128,16384]{1,0:T(8,128)} %weight_ref.10, f32[128,1]{1,0:T(8,128)} %copy.80.gain_ref), custom_call_target="tpu_custom_call" | custom-call | flops 1048576 | bytes 6291456 | tf_op jit(solution)/shard_map/pallas_call | solution.py:44
  211.3 23.8 %collective-permute-done.5 = bf16[1,8,2,256,128]{4,3,2,1,0:T(8,128)(2,1)S(1)} collective-permute-done((bf16[1,8,2,256,128]{4,3,2,1,0:T(8,128)(2,1)S(1)}, bf16[1,8,2,256,128]{4,3,2,1,0:T(8,128)(2,1)S(1)}, u32[]{:S(2)}, u32[]{:S(2)}) %collective-permute-start.5) | collective-permute-done | bytes 1048608 | tf_op jit(solution)/shard_map/ppermute | solution.py:63
  236.2 6.5 %all-to-all-done.4.gate_ref = bf16[16,2,256,128]{3,2,1,0:T(8,128)(2,1)S(1)} async-done(((bf16[16,2,256,128]{3,2,1,0:T(8,128)(2,1)}), bf16[16,2,256,128]{3,2,1,0:T(8,128)(2,1)S(1)}, u32[]{:S(2)}, u32[]{:S(2)}) %all-to-all-start.4) | async-done | bytes 2097184 | tf_op jit(solution)/shard_map/all_to_all | solution.py:251
  244.1 11.3 %all-to-all-start.2 = ((bf16[16,2,256,128]{3,2,1,0:T(8,128)(2,1)}), bf16[16,2,256,128]{3,2,1,0:T(8,128)(2,1)}, u32[]{:S(2)}, u32[]{:S(2)}) async-start(bf16[16,2,256,128]{3,2,1,0:T(8,128)(2,1)} %bitcast.40), calls=%async_computation.2 | async-start | bytes 4194304 | tf_op jit(solution)/shard_map/all_to_all | solution.py:251
  255.4 6.9 %shard_map.153 = bf16[2,8,2,256,128]{4,3,2,1,0:T(8,128)(2,1)} custom-call(f32[128,16384]{1,0:T(8,128)} %weight_ref.8, f32[128,1]{1,0:T(8,128)} %copy.80.gain_ref), custom_call_target="tpu_custom_call" | custom-call | flops 1048576 | bytes 6291456 | tf_op jit(solution)/shard_map/pallas_call | solution.py:44
  276.3 14.6 %collective-permute-done = bf16[1,8,2,256,128]{4,3,2,1,0:T(8,128)(2,1)} collective-permute-done((bf16[1,8,2,256,128]{4,3,2,1,0:T(8,128)(2,1)}, bf16[1,8,2,256,128]{4,3,2,1,0:T(8,128)(2,1)}, u32[]{:S(2)}, u32[]{:S(2)}) %collective-permute-start) | collective-permute-done | bytes 1048608 | tf_op jit(solution)/shard_map/ppermute | solution.py:63
  293.3 8.2 %collective-permute-done.1 = bf16[1,128,1024]{2,0,1:T(2,128)(2,1)S(1)} collective-permute-done((bf16[1,128,1024]{2,0,1:T(2,128)(2,1)S(1)}, bf16[1,128,1024]{2,0,1:T(2,128)(2,1)S(1)}, u32[]{:S(2)}, u32[]{:S(2)}) %collective-permute-start.1) | collective-permute-done | bytes 262176 | tf_op jit(solution)/shard_map/ppermute | solution.py:63
  308.4 6.3 %slice_reduce_fusion.11 = (s32[16,128]{1,0:T(8,128)S(1)}, s32[16,128]{1,0:T(8,128)S(1)}, s32[16,128]{1,0:T(8,128)S(1)}, s32[16,128]{1,0:T(8,128)S(1)}, s32[16,12...) fusion(s32[16,128,128]{2,1,0:T(8,128)S(1)} %slice_convert_fusion), kind=kLoop, calls=%fused_computation.31 | loop fusion | bytes 196608 | tf_op jit(solution)/shard_map/slice | solution.py:199
  317.8 4.8 shard_map.156
  322.5 5.7 %all-to-all-start.5 = ((bf16[16,2,256,128]{3,2,1,0:T(8,128)(2,1)}), bf16[16,2,256,128]{3,2,1,0:T(8,128)(2,1)S(1)}, u32[]{:S(2)}, u32[]{:S(2)}) async-start(bf16[16,2,256,128]{3,2,1,0:T(8,128)(2,1)} %bitcast.1), calls=%async_computation.5 | async-start | bytes 4194304 | tf_op jit(solution)/shard_map/all_to_all | solution.py:251
  328.3 6.6 %shard_map.157 = bf16[2,8,2,256,128]{4,3,2,1,0:T(8,128)(2,1)} custom-call(f32[128,16384]{1,0:T(8,128)} %weight_ref.10, f32[128,1]{1,0:T(8,128)} %copy.80.gain_ref), custom_call_target="tpu_custom_call" | custom-call | flops 1048576 | bytes 6291456 | tf_op jit(solution)/shard_map/pallas_call | solution.py:44
  337.8 23.8 %collective-permute-done.4 = bf16[1,8,2,256,128]{4,3,2,1,0:T(8,128)(2,1)S(1)} collective-permute-done((bf16[1,8,2,256,128]{4,3,2,1,0:T(8,128)(2,1)S(1)}, bf16[1,8,2,256,128]{4,3,2,1,0:T(8,128)(2,1)S(1)}, u32[]{:S(2)}, u32[]{:S(2)}) %collective-permute-start.4) | collective-permute-done | bytes 1048608 | tf_op jit(solution)/shard_map/ppermute | solution.py:63
  370.6 11.3 %all-to-all-start.6 = ((bf16[16,2,256,128]{3,2,1,0:T(8,128)(2,1)}), bf16[16,2,256,128]{3,2,1,0:T(8,128)(2,1)}, u32[]{:S(2)}, u32[]{:S(2)}) async-start(bf16[16,2,256,128]{3,2,1,0:T(8,128)(2,1)} %bitcast.39), calls=%async_computation.6 | async-start | bytes 4194304 | tf_op jit(solution)/shard_map/all_to_all | solution.py:251
  385.0 23.8 %collective-permute-done.6 = bf16[1,16,2,16,1024]{4,3,2,1,0:T(8,128)(2,1)S(1)} collective-permute-done((bf16[1,16,2,16,1024]{4,3,2,1,0:T(8,128)(2,1)S(1)}, bf16[1,16,2,16,1024]{4,3,2,1,0:T(8,128)(2,1)S(1)}, u32[]{:S(2)}, u32[]{:S(2)}) %collective-permute-start.6) | collective-permute-done | bytes 1048608 | tf_op jit(solution)/shard_map/ppermute | solution.py:63
  410.7 12.2 %all-to-all-done.6.down_ref = bf16[16,2,256,128]{3,2,1,0:T(8,128)(2,1)} async-done(((bf16[16,2,256,128]{3,2,1,0:T(8,128)(2,1)}), bf16[16,2,256,128]{3,2,1,0:T(8,128)(2,1)}, u32[]{:S(2)}, u32[]{:S(2)}) %all-to-all-start.6) | async-done | bytes 2097184 | tf_op jit(solution)/shard_map/all_to_all | solution.py:251
  422.9 11.3 %all-to-all-start.3 = ((bf16[16,2,16,1024]{3,2,1,0:T(8,128)(2,1)}), bf16[16,2,16,1024]{3,2,1,0:T(8,128)(2,1)}, u32[]{:S(2)}, u32[]{:S(2)}) async-start(bf16[16,2,16,1024]{3,2,1,0:T(8,128)(2,1)} %reduce_sum.57), calls=%async_computation.3 | async-start | bytes 2097152 | tf_op jit(solution)/shard_map/all_to_all | solution.py:226
  434.1 4.6 fusion.4
  440.3 4.8 shard_map.161
  451.9 23.8 %collective-permute-done.8 = bf16[1,16,2,16,1024]{4,3,2,1,0:T(8,128)(2,1)S(1)} collective-permute-done((bf16[1,16,2,16,1024]{4,3,2,1,0:T(8,128)(2,1)S(1)}, bf16[1,16,2,16,1024]{4,3,2,1,0:T(8,128)(2,1)S(1)}, u32[]{:S(2)}, u32[]{:S(2)}) %collective-permute-start.8) | collective-permute-done | bytes 1048608 | tf_op jit(solution)/shard_map/ppermute | solution.py:63
  480.3 5.9 %all-to-all-start.7 = ((bf16[16,2,16,1024]{3,2,1,0:T(8,128)(2,1)}), bf16[16,2,16,1024]{3,2,1,0:T(8,128)(2,1)}, u32[]{:S(2)}, u32[]{:S(2)}) async-start(bf16[16,2,16,1024]{3,2,1,0:T(8,128)(2,1)} %reduce_sum.58), calls=%async_computation.7 | async-start | bytes 2097152 | tf_op jit(solution)/shard_map/all_to_all | solution.py:226
  496.2 12.9 %all-to-all-done.7 = bf16[16,2,16,1024]{3,2,1,0:T(8,128)(2,1)} async-done(((bf16[16,2,16,1024]{3,2,1,0:T(8,128)(2,1)}), bf16[16,2,16,1024]{3,2,1,0:T(8,128)(2,1)}, u32[]{:S(2)}, u32[]{:S(2)}) %all-to-all-start.7) | async-done | bytes 1048608 | tf_op jit(solution)/shard_map/all_to_all | solution.py:226
  (120 shorter events, 102.2 us)
Async XLA Ops:
  7.2 7.1 %copy-start.11 = (bf16[128,2048]{1,0:T(8,128)(2,1)S(1)}, bf16[128,2048]{1,0:T(8,128)(2,1)}, u32[]{:S(2)}) copy-start(bf16[128,2048]{1,0:T(8,128)(2,1)} %param.10) | copy-start | bytes 1572868
  7.2 259.0 %all-gather.3.cloned.1.call-start = ((), (), s32[]{:S(2)}) async-start(), calls=%async_computation.8 | async-start | bytes 3342336 | tf_op jit(solution)/shard_map/all_gather | solution.py:214
  9.3 7.0 %copy-start.15 = (f32[128]{0:T(128)S(1)}, f32[128]{0:T(128)}, u32[]{:S(2)}) copy-start(f32[128]{0:T(128)} %param.11) | copy-start | bytes 1540
  11.7 295.5 %all-gather.5.cloned.1.call-start = ((), (), s32[]{:S(2)}) async-start(), calls=%async_computation.9 | async-start | bytes 9191424 | tf_op jit(solution)/shard_map/all_gather | solution.py:188
  25.2 26.2 %collective-permute-start.2 = (bf16[1,8,2,256,128]{4,3,2,1,0:T(8,128)(2,1)S(1)}, bf16[1,8,2,256,128]{4,3,2,1,0:T(8,128)(2,1)S(1)}, u32[]{:S(2)}, u32[]{:S(2)}) collective-permute-start(bf16[1,8,2,256,128]{4,3,2,1,0:T(8,128)(2,1)S(1)} %constant_dynamic-slice_fusion.6), channel_id=1, source_target_pairs={{0,1},{1,0},{2,3},{3,2},{4,5},{5,4},{6,7},{7,6},{8,9},{9,8},{10,11... | collective-permute-start | bytes 3145736 | tf_op jit(solution)/shard_map/ppermute | solution.py:63
  52.5 55.9 %all-to-all-start = ((bf16[16,2,256,128]{3,2,1,0:T(8,128)(2,1)}), bf16[16,2,256,128]{3,2,1,0:T(8,128)(2,1)S(1)}, u32[]{:S(2)}, u32[]{:S(2)}) async-start(bf16[16,2,256,128]{3,2,1,0:T(8,128)(2,1)} %bitcast.19), calls=%async_computation | async-start | bytes 4194304 | tf_op jit(solution)/shard_map/all_to_all | solution.py:251
  66.8 27.5 %collective-permute-start.3 = (bf16[1,8,2,256,128]{4,3,2,1,0:T(8,128)(2,1)S(1)}, bf16[1,8,2,256,128]{4,3,2,1,0:T(8,128)(2,1)S(1)}, u32[]{:S(2)}, u32[]{:S(2)}) collective-permute-start(bf16[1,8,2,256,128]{4,3,2,1,0:T(8,128)(2,1)S(1)} %constant_dynamic-slice_fusion.5), channel_id=1, source_target_pairs={{0,1},{1,0},{2,3},{3,2},{4,5},{5,4},{6,7},{7,6},{8,9},{9,8},{10,11... | collective-permute-start | bytes 3145736 | tf_op jit(solution)/shard_map/ppermute | solution.py:63
  109.6 81.1 %all-to-all-start.1 = ((bf16[16,2,256,128]{3,2,1,0:T(8,128)(2,1)}), bf16[16,2,256,128]{3,2,1,0:T(8,128)(2,1)}, u32[]{:S(2)}, u32[]{:S(2)}) async-start(bf16[16,2,256,128]{3,2,1,0:T(8,128)(2,1)} %bitcast.20), calls=%async_computation.1 | async-start | bytes 4194304 | tf_op jit(solution)/shard_map/all_to_all | solution.py:251
  138.3 28.6 %collective-permute-start.7 = (bf16[1,8,2,256,128]{4,3,2,1,0:T(8,128)(2,1)S(1)}, bf16[1,8,2,256,128]{4,3,2,1,0:T(8,128)(2,1)S(1)}, u32[]{:S(2)}, u32[]{:S(2)}) collective-permute-start(bf16[1,8,2,256,128]{4,3,2,1,0:T(8,128)(2,1)S(1)} %constant_dynamic-slice_fusion.1), channel_id=1, source_target_pairs={{0,1},{1,0},{2,3},{3,2},{4,5},{5,4},{6,7},{7,6},{8,9},{9,8},{10,11... | collective-permute-start | bytes 3145736 | tf_op jit(solution)/shard_map/ppermute | solution.py:63
  190.8 51.9 %all-to-all-start.4 = ((bf16[16,2,256,128]{3,2,1,0:T(8,128)(2,1)}), bf16[16,2,256,128]{3,2,1,0:T(8,128)(2,1)S(1)}, u32[]{:S(2)}, u32[]{:S(2)}) async-start(bf16[16,2,256,128]{3,2,1,0:T(8,128)(2,1)} %bitcast.45), calls=%async_computation.4 | async-start | bytes 4194304 | tf_op jit(solution)/shard_map/all_to_all | solution.py:251
  209.6 25.5 %collective-permute-start.5 = (bf16[1,8,2,256,128]{4,3,2,1,0:T(8,128)(2,1)S(1)}, bf16[1,8,2,256,128]{4,3,2,1,0:T(8,128)(2,1)S(1)}, u32[]{:S(2)}, u32[]{:S(2)}) collective-permute-start(bf16[1,8,2,256,128]{4,3,2,1,0:T(8,128)(2,1)S(1)} %constant_dynamic-slice_fusion.3), channel_id=1, source_target_pairs={{0,1},{1,0},{2,3},{3,2},{4,5},{5,4},{6,7},{7,6},{8,9},{9,8},{10,11... | collective-permute-start | bytes 3145736 | tf_op jit(solution)/shard_map/ppermute | solution.py:63
  242.7 1.4 copy-start.5
  244.1 78.5 %all-to-all-start.2 = ((bf16[16,2,256,128]{3,2,1,0:T(8,128)(2,1)}), bf16[16,2,256,128]{3,2,1,0:T(8,128)(2,1)}, u32[]{:S(2)}, u32[]{:S(2)}) async-start(bf16[16,2,256,128]{3,2,1,0:T(8,128)(2,1)} %bitcast.40), calls=%async_computation.2 | async-start | bytes 4194304 | tf_op jit(solution)/shard_map/all_to_all | solution.py:251
  264.6 26.3 %collective-permute-start = (bf16[1,8,2,256,128]{4,3,2,1,0:T(8,128)(2,1)}, bf16[1,8,2,256,128]{4,3,2,1,0:T(8,128)(2,1)}, u32[]{:S(2)}, u32[]{:S(2)}) collective-permute-start(bf16[1,8,2,256,128]{4,3,2,1,0:T(8,128)(2,1)} %constant_dynamic-slice_fusion.7), channel_id=1, source_target_pairs={{0,1},{1,0},{2,3},{3,2},{4,5},{5,4},{6,7},{7,6},{8,9},{9,8},{10,11... | collective-permute-start | bytes 3145736 | tf_op jit(solution)/shard_map/ppermute | solution.py:63
  269.4 2.6 copy-start.9
  271.0 1.6 copy-start.1
  275.9 25.5 %collective-permute-start.1 = (bf16[1,128,1024]{2,0,1:T(2,128)(2,1)S(1)}, bf16[1,128,1024]{2,0,1:T(2,128)(2,1)S(1)}, u32[]{:S(2)}, u32[]{:S(2)}) collective-permute-start(bf16[1,128,1024]{2,0,1:T(2,128)(2,1)S(1)} %dynamic-slice_bitcast_fusion), channel_id=1, source_target_pairs={{0,1},{1,0},{2,3},{3,2},{4,5},{5,4},{6,7},{7,6},{8,9},{9,8},{10,11... | collective-permute-start | bytes 786440 | tf_op jit(solution)/shard_map/ppermute | solution.py:63
  308.4 6.6 %copy-start = (bf16[2048,2176]{1,0:T(8,128)(2,1)S(1)}, bf16[2048,2176]{1,0:T(8,128)(2,1)}, u32[]{:S(2)}) copy-start(bf16[2048,2176]{1,0:T(8,128)(2,1)} %all-gather.5.cloned.1.call-done) | copy-start | bytes 26738692
  322.5 46.7 %all-to-all-start.5 = ((bf16[16,2,256,128]{3,2,1,0:T(8,128)(2,1)}), bf16[16,2,256,128]{3,2,1,0:T(8,128)(2,1)S(1)}, u32[]{:S(2)}, u32[]{:S(2)}) async-start(bf16[16,2,256,128]{3,2,1,0:T(8,128)(2,1)} %bitcast.1), calls=%async_computation.5 | async-start | bytes 4194304 | tf_op jit(solution)/shard_map/all_to_all | solution.py:251
  336.1 25.5 %collective-permute-start.4 = (bf16[1,8,2,256,128]{4,3,2,1,0:T(8,128)(2,1)S(1)}, bf16[1,8,2,256,128]{4,3,2,1,0:T(8,128)(2,1)S(1)}, u32[]{:S(2)}, u32[]{:S(2)}) collective-permute-start(bf16[1,8,2,256,128]{4,3,2,1,0:T(8,128)(2,1)S(1)} %constant_dynamic-slice_fusion.4), channel_id=1, source_target_pairs={{0,1},{1,0},{2,3},{3,2},{4,5},{5,4},{6,7},{7,6},{8,9},{9,8},{10,11... | collective-permute-start | bytes 3145736 | tf_op jit(solution)/shard_map/ppermute | solution.py:63
  369.2 1.3 copy-start.7
  370.6 52.3 %all-to-all-start.6 = ((bf16[16,2,256,128]{3,2,1,0:T(8,128)(2,1)}), bf16[16,2,256,128]{3,2,1,0:T(8,128)(2,1)}, u32[]{:S(2)}, u32[]{:S(2)}) async-start(bf16[16,2,256,128]{3,2,1,0:T(8,128)(2,1)} %bitcast.39), calls=%async_computation.6 | async-start | bytes 4194304 | tf_op jit(solution)/shard_map/all_to_all | solution.py:251
  381.8 27.0 %copy-start.10 = (bf16[2,16,2,16,1024]{4,3,2,1,0:T(8,128)(2,1)S(1)}, bf16[2,16,2,16,1024]{4,3,2,1,0:T(8,128)(2,1)}, u32[]{:S(2)}) copy-start(bf16[2,16,2,16,1024]{4,3,2,1,0:T(8,128)(2,1)} %get-tuple-element.24) | copy-start | bytes 6291460
  383.3 25.5 %collective-permute-start.6 = (bf16[1,16,2,16,1024]{4,3,2,1,0:T(8,128)(2,1)S(1)}, bf16[1,16,2,16,1024]{4,3,2,1,0:T(8,128)(2,1)S(1)}, u32[]{:S(2)}, u32[]{:S(2)}) collective-permute-start(bf16[1,16,2,16,1024]{4,3,2,1,0:T(8,128)(2,1)S(1)} %constant_dynamic-slice_fusion.2), channel_id=1, source_target_pairs={{0,1},{1,0},{2,3},{3,2},{4,5},{5,4},{6,7},{7,6},{8,9},{9,8},{10,11... | collective-permute-start | bytes 3145736 | tf_op jit(solution)/shard_map/ppermute | solution.py:63
  422.9 57.4 %all-to-all-start.3 = ((bf16[16,2,16,1024]{3,2,1,0:T(8,128)(2,1)}), bf16[16,2,16,1024]{3,2,1,0:T(8,128)(2,1)}, u32[]{:S(2)}, u32[]{:S(2)}) async-start(bf16[16,2,16,1024]{3,2,1,0:T(8,128)(2,1)} %reduce_sum.57), calls=%async_computation.3 | async-start | bytes 2097152 | tf_op jit(solution)/shard_map/all_to_all | solution.py:226
  450.2 25.5 %collective-permute-start.8 = (bf16[1,16,2,16,1024]{4,3,2,1,0:T(8,128)(2,1)S(1)}, bf16[1,16,2,16,1024]{4,3,2,1,0:T(8,128)(2,1)S(1)}, u32[]{:S(2)}, u32[]{:S(2)}) collective-permute-start(bf16[1,16,2,16,1024]{4,3,2,1,0:T(8,128)(2,1)S(1)} %constant_dynamic-slice_fusion), channel_id=1, source_target_pairs={{0,1},{1,0},{2,3},{3,2},{4,5},{5,4},{6,7},{7,6},{8,9},{9,8},{10,11... | collective-permute-start | bytes 3145736 | tf_op jit(solution)/shard_map/ppermute | solution.py:63
  476.7 9.5 %copy-start.14 = (f32[128,6]{0,1:T(8,128)S(1)}, f32[128,6]{0,1:T(8,128)}, u32[]{:S(2)}) copy-start(f32[128,6]{0,1:T(8,128)} %param.19) | copy-start | bytes 9220
  476.7 9.5 %copy-start.13 = (s32[128,6]{0,1:T(8,128)S(1)}, s32[128,6]{0,1:T(8,128)}, u32[]{:S(2)}) copy-start(s32[128,6]{0,1:T(8,128)} %param.18) | copy-start | bytes 9220
  476.8 9.5 %copy-start.4 = (bf16[256,16,128]{0,2,1:T(8,128)(2,1)S(1)}, bf16[256,16,128]{0,2,1:T(8,128)(2,1)}, u32[]{:S(2)}) copy-start(bf16[256,16,128]{0,2,1:T(8,128)(2,1)} %copy-done.3) | copy-start | bytes 3145732
  480.2 7.4 %copy-start.2 = (bf16[256,16,128]{0,2,1:T(8,128)(2,1)S(1)}, bf16[256,16,128]{0,2,1:T(8,128)(2,1)}, u32[]{:S(2)}) copy-start(bf16[256,16,128]{0,2,1:T(8,128)(2,1)} %get-tuple-element.63) | copy-start | bytes 3145732
  480.3 28.9 %all-to-all-start.7 = ((bf16[16,2,16,1024]{3,2,1,0:T(8,128)(2,1)}), bf16[16,2,16,1024]{3,2,1,0:T(8,128)(2,1)}, u32[]{:S(2)}, u32[]{:S(2)}) async-start(bf16[16,2,16,1024]{3,2,1,0:T(8,128)(2,1)} %reduce_sum.58), calls=%async_computation.7 | async-start | bytes 2097152 | tf_op jit(solution)/shard_map/all_to_all | solution.py:226
  490.5 1.9 copy-start.12
  (3 other events, 3.1 us)
Sparse Core Ops, SparseCore 0:
  11.8 48.3 all-gather.2
  63.1 124.1 all-gather.4
